TPU v7x, 32 devices: a whole 2x2x4 slice. The times are simulated.
32 devices in a mesh: ep: 4 (over y, x), tp: 8 (over z, core).
Axes of the slice: x: 2, y: 2, z: 4, core: 2. Of those that a mesh axis runs over, the one named last changes fastest.
Arguments:
- tokens: bfloat16 [64, 4096], P(None, 'ep'), may hold values from -60 to 60
- gain_attn: bfloat16 [4096], P('ep'), may hold values from 0.099609375 to 1.8984375
- w_query: bfloat16 [4096, 2048], P('ep', 'tp'), may hold values from -0.09375 to 0.09375
- w_key: bfloat16 [4096, 2048], P('ep', 'tp'), may hold values from -0.09375 to 0.09375
- w_value: bfloat16 [4096, 2048], P('ep', 'tp'), may hold values from -0.09375 to 0.09375
- w_output: bfloat16 [2048, 4096], P('tp', 'ep'), may hold values from -0.125 to 0.125
- key_cache: bfloat16 [64, 1024, 2048], P('ep', None, 'tp'), may hold values from -6 to 6
- value_cache: bfloat16 [64, 1024, 2048], P('ep', None, 'tp'), may hold values from -10 to 10
- lengths: int32 [64], P('ep'), may hold values from 128 to 1024
- score_shift: float32 [16], P('tp'), may hold values from -9.5 to -3.5
- gain_ffn: bfloat16 [4096], replicated, may hold values from 0.099609375 to 1.8984375
- w_mix: bfloat16 [4096], P('ep'), may hold values from -0.09375 to 0.09375
- w_dense_gate: bfloat16 [4096, 4096], P('ep', 'tp'), may hold values from -0.09375 to 0.09375
- w_dense_up: bfloat16 [4096, 4096], P('ep', 'tp'), may hold values from -0.09375 to 0.09375
- w_dense_down: bfloat16 [4096, 4096], P('tp', 'ep'), may hold values from -0.09375 to 0.09375
- route_group: int32 [64], replicated, may hold values from 0 to 3, as said below
- route_inner: int32 [64, 2], replicated, may hold values from 0 to 3, as said below
- route_weight: float32 [64, 2], replicated, may hold values from 0.3 to 1
- w_exp_gate: bfloat16 [16, 4096, 2048], P('ep', None, 'tp'), may hold values from -0.09375 to 0.09375
- w_exp_up: bfloat16 [16, 4096, 2048], P('ep', None, 'tp'), may hold values from -0.09375 to 0.09375
- w_exp_down: bfloat16 [16, 2048, 4096], P('ep', 'tp'), may hold values from -0.125 to 0.125
Outputs:
- mixed: bfloat16 [64, 4096], P(None, 'ep')
- new_keys: bfloat16 [64, 2048], P('ep', 'tp')
- new_values: bfloat16 [64, 2048], P('ep', 'tp')
Inputs may be any that keep to these rules, and one draw needn't show every extreme that they name: `route_group`: within every aligned block of 16 sequences (the sequences of one index of ep) exactly half of the tokens use one group, the same group in every block; the other groups share the rest. A token's 2 experts inside its group differ. Within every aligned block of 16 sequences no expert (route_group * 4 + route_inner) is used by more than 4 tokens, and the experts of the group that half of the block uses are each used by exactly 4.
All inputs are finite; a program needn't handle non-finite values.
Results may differ from a plain program's by a relative error of at most 0.0039.
The roundings to bfloat16 on the way count: a program that leaves them out, or rounds other values in their place, can miss the bound.
Values may be sent and summed in bfloat16 or wider, within the bound.
A program may use at most 128 MiB of HBM per device.

v0:
```python
import math
import jax
import jax.numpy as jnp
from jax import lax
from jax.sharding import PartitionSpec as P

D = 4096
HD = 128
EPG = 4
TOPK = 2
EXPERTS = 16
CAP = 4
norm_eps = 1e-06


def on_device(
    tokens,
    gain_attn,
    w_query,
    w_key,
    w_value,
    w_output,
    key_cache,
    value_cache,
    lengths,
    score_shift,
    gain_ffn,
    w_mix,
    w_dense_gate,
    w_dense_up,
    w_dense_down,
    route_group,
    route_inner,
    route_weight,
    w_exp_gate,
    w_exp_up,
    w_exp_down,
):
    ep_count = lax.axis_size("ep")
    batch_all, col_width = tokens.shape
    seq_local = batch_all // ep_count
    head_cols = w_query.shape[1]
    heads_local = head_cols // HD
    tokens_float = tokens.astype(jnp.float32)
    squares = lax.psum_scatter(
        jnp.sum(tokens_float * tokens_float, axis=1), "ep", scatter_dimension=0, tiled=True
    )
    inv_first = lax.rsqrt(squares / D + norm_eps)[:, None]
    scaled_in = (tokens_float * gain_attn.astype(jnp.float32)).astype(jnp.bfloat16)
    w_joint = jnp.concatenate([w_query, w_key, w_value], axis=1)
    joint_proj = (
        lax.psum_scatter(
            jnp.dot(scaled_in, w_joint, preferred_element_type=jnp.float32),
            "ep",
            scatter_dimension=0,
            tiled=True,
        )
        * inv_first
    )
    queries = joint_proj[:, :head_cols].astype(jnp.bfloat16)
    new_keys = joint_proj[:, head_cols : 2 * head_cols].astype(jnp.bfloat16)
    new_values = joint_proj[:, 2 * head_cols :].astype(jnp.bfloat16)
    cache_len = key_cache.shape[1]
    head_query = queries.reshape(seq_local, heads_local, HD)
    head_keys = key_cache.reshape(seq_local, cache_len, heads_local, HD)
    scores = jnp.einsum(
        "bhd,blhd->bhl", head_query, head_keys, preferred_element_type=jnp.float32
    ) / math.sqrt(HD)
    scores = scores + score_shift[None, :, None]
    live_mask = lax.broadcasted_iota(jnp.int32, scores.shape, 2) < lengths[:, None, None]
    soft_terms = jnp.where(live_mask, jax.nn.softplus(scores), 0.0)
    later_sum = lax.cumsum(soft_terms, axis=2, reverse=True) - soft_terms
    stick = jnp.where(live_mask, jnp.exp(jax.nn.log_sigmoid(scores) - later_sum), 0.0).astype(
        jnp.bfloat16
    )
    head_values = value_cache.reshape(seq_local, cache_len, heads_local, HD)
    attended = jnp.einsum("bhl,blhd->bhd", stick, head_values, preferred_element_type=jnp.float32)
    attended = attended.reshape(seq_local, head_cols).astype(jnp.bfloat16)
    attn_part = jnp.dot(
        lax.all_gather(attended, "ep", axis=0, tiled=True),
        w_output,
        preferred_element_type=jnp.float32,
    )
    attn_out = lax.psum(attn_part, "tp")
    middle = (tokens_float + attn_out).astype(jnp.bfloat16)
    middle_float = middle.astype(jnp.float32)
    gain_float = gain_ffn.astype(jnp.float32)
    gain_cols = lax.dynamic_slice_in_dim(gain_float, lax.axis_index("ep") * col_width, col_width, 0)
    scaled_mid = (middle_float * gain_cols).astype(jnp.bfloat16)
    dense_pre, dense_lin, mix_pre, mid_squares = lax.psum(
        (
            jnp.dot(scaled_mid, w_dense_gate, preferred_element_type=jnp.float32),
            jnp.dot(scaled_mid, w_dense_up, preferred_element_type=jnp.float32),
            jnp.dot(scaled_mid, w_mix, preferred_element_type=jnp.float32),
            jnp.sum(middle_float * middle_float, axis=1),
        ),
        "ep",
    )
    inv_second = lax.rsqrt(mid_squares / D + norm_eps)[:, None]
    dense_hidden = (jax.nn.silu(dense_pre * inv_second) * (dense_lin * inv_second)).astype(
        jnp.bfloat16
    )
    mix_gate = jax.nn.sigmoid(mix_pre * inv_second[:, 0])
    dense_part = (
        jnp.dot(dense_hidden, w_dense_down, preferred_element_type=jnp.float32) * mix_gate[:, None]
    )
    slot_count = CAP * ep_count
    expert_ids = (route_group[:, None] * EPG + route_inner).reshape(-1)
    expert_onehot = (expert_ids[:, None] == jnp.arange(EXPERTS, dtype=jnp.int32)[None, :]).astype(
        jnp.int32
    )
    per_block = expert_onehot.reshape(ep_count, seq_local * TOPK, EXPERTS)
    earlier = (jnp.cumsum(per_block, axis=1) - per_block).reshape(-1, EXPERTS)
    slot_rank = jnp.sum(earlier * expert_onehot, axis=1)
    route_index = jnp.arange(batch_all * TOPK, dtype=jnp.int32)
    block_of = route_index // (seq_local * TOPK)
    slot_flat = expert_ids * slot_count + block_of * CAP + slot_rank
    slot_table = (
        jnp.full((EXPERTS * slot_count,), batch_all, jnp.int32)
        .at[slot_flat]
        .set(route_index // TOPK)
    )
    padded_middle = jnp.concatenate([middle, jnp.zeros((1, col_width), jnp.bfloat16)], axis=0)
    outgoing = jnp.take(padded_middle, slot_table, axis=0).reshape(EXPERTS, slot_count, col_width)
    arrived_float = lax.all_to_all(outgoing, "ep", split_axis=0, concat_axis=2, tiled=True).astype(
        jnp.float32
    )
    inv_rows = lax.rsqrt(jnp.mean(arrived_float * arrived_float, axis=2, keepdims=True) + norm_eps)
    scaled_rows = (arrived_float * gain_float).astype(jnp.bfloat16)
    gate_pre = (
        jnp.einsum("end,edf->enf", scaled_rows, w_exp_gate, preferred_element_type=jnp.float32)
        * inv_rows
    )
    up_proj = (
        jnp.einsum("end,edf->enf", scaled_rows, w_exp_up, preferred_element_type=jnp.float32)
        * inv_rows
    )
    hidden = (jax.nn.silu(gate_pre) * up_proj).astype(jnp.bfloat16)
    expert_rows = jnp.einsum("enf,efd->end", hidden, w_exp_down, preferred_element_type=jnp.float32)
    returned = lax.all_to_all(expert_rows, "ep", split_axis=2, concat_axis=0, tiled=True)
    flat_back = returned.reshape(EXPERTS * slot_count, col_width)
    routed = jnp.take(flat_back, slot_flat, axis=0).reshape(batch_all, TOPK, col_width)
    expert_part = jnp.sum(routed * route_weight[:, :, None], axis=1)
    result_sum = middle_float + lax.psum(expert_part + dense_part, "tp")
    return (result_sum.astype(jnp.bfloat16), new_keys, new_values)


def solution(mesh):
    placed = (
        P(None, "ep"),
        P("ep"),
        P("ep", "tp"),
        P("ep", "tp"),
        P("ep", "tp"),
        P("tp", "ep"),
        P("ep", None, "tp"),
        P("ep", None, "tp"),
        P("ep"),
        P("tp"),
        P(),
        P("ep"),
        P("ep", "tp"),
        P("ep", "tp"),
        P("tp", "ep"),
        P(),
        P(),
        P(),
        P("ep", None, "tp"),
        P("ep", None, "tp"),
        P("ep", "tp", None),
    )
    return jax.shard_map(
        on_device,
        mesh=mesh,
        in_specs=placed,
        out_specs=(P(None, "ep"), P("ep", "tp"), P("ep", "tp")),
        check_vma=False,
    )
```

profile of v0, /device:TPU:0, one launch (start us, length us, event | category | flops | bytes accessed | tf_op | source)
XLA Modules:
  0.0 316.2 jit_solution(12506751394663622789)
XLA Ops:
  7.2 0.8 convert_element_type.69
  8.0 2.5 fusion.3
  10.6 1.0 fusion.14
  11.7 12.3 %copy.64 = bf16[16,1024,256]{1,2,0:T(8,128)(2,1)} copy(bf16[16,1024,256]{2,1,0:T(8,128)(2,1)} %param.27) | data formatting | bytes 16777216 | tf_op jit(solution)/shard_map/reshape | solution.py:65
  24.0 0.1 copy.50
  24.1 0.1 eq.19
  24.2 0.1 fusion.41
  24.3 0.1 reduce_window_sum.27
  24.4 0.2 select_reduce_fusion
  24.6 0.1 reduce_sum.59
  24.7 0.1 copy.53
  24.8 0.1 mul.169
  24.9 0.6 dynamic-slice
  26.2 1.0 scatter_custom_fusion
  27.2 11.5 %all-reduce.1 = f32[64]{0:T(128)S(1)} all-reduce(f32[64]{0:T(128)S(1)} %fusion.14), channel_id=3, replica_groups=mesh['ep'=4,'tp'=8] {'ep'}, use_global_device_ids=true, to_apply=%region_2.0.clone | all-reduce | flops 64 | bytes 512
  38.7 0.1 fusion.52
  38.8 0.9 multiply_convert_fusion.6
  39.7 0.6 fusion.57
  40.3 4.6 %fusion.58 = f32[16,2,1,1024]{3,2,1,0:T(1,128)S(1)} fusion(bf16[16,2,128,1]{2,3,1,0:T(2,128)(2,1)S(1)} %reshape.226, bf16[16,1024,2,128]{1,3,2,0:T(8,128)(2,1)} %bitcast.59), kind=kOutput, calls=%fused_computation.104 | convolution fusion | flops 8388608 | bytes 8527872 | tf_op jit(solution)/shard_map/bhd,blhd->bhl/dot_general | solution.py:66
  44.9 0.4 fusion.24
  45.3 0.1 reshape.188
  45.4 39.6 %reduce-window.6 = f32[16,2,8,128]{3,2,1,0:T(8,128)S(1)} reduce-window(f32[16,2,8,128]{3,2,1,0:T(8,128)S(1)} %reshape.188, f32[]{:T(128)} %constant.94.clone.1), window={size=1x1x1x128 pad=0_0x0_0x0_0x0_127}, to_apply=%region_3.4 | reduce-window | flops 4161536 | bytes 262148 | tf_op jit(solution)/shard_map/reduce-window
  85.0 0.2 copy.48
  85.3 0.1 copy.49
  85.3 0.1 broadcast_add_fusion
  85.4 0.1 reduce_window_sum.26
  85.5 0.8 fusion.42
  86.4 4.6 %fusion = f32[16,2,1,128]{3,2,1,0:T(1,128)S(1)} fusion(bf16[16,2,1024,1]{2,1,0,3:T(2,128)(2,1)S(1)} %fusion.42, bf16[16,1024,256]{2,1,0:T(8,128)(2,1)} %param.28), kind=kOutput, calls=%fused_computation.3 | convolution fusion | flops 8388608 | bytes 8470528 | tf_op jit(solution)/shard_map/bhl,blhd->bhd/dot_general | solution.py:77
  91.0 7.1 %all_gather.3 = bf16[64,256]{1,0:T(8,128)(2,1)S(1)} all-gather(bf16[16,256]{1,0:T(8,128)(2,1)S(1)} %bitcast.70), channel_id=1, replica_groups=mesh['ep'=4,'tp'=8] {'ep'}, dimensions={0}, use_global_device_ids=true | all-gather | bytes 40960 | tf_op jit(solution)/shard_map/all_gather | solution.py:80
  98.1 0.9 fusion.59
  99.1 0.1 broadcast_in_dim.46
  99.2 55.8 %all-reduce.8.cloned.1.call-done = f32[64,1024]{1,0:T(8,128)} async-done(((f32[64,1024]{1,0:T(8,128)}), f32[64,1024]{1,0:T(8,128)}) %all-reduce.8.cloned.1.call-update) | async-done | bytes 262160 | tf_op jit(solution)/shard_map/psum | solution.py:84
  154.9 1.1 fusion.17
  156.0 1.2 gather_fusion
  157.2 0.9 broadcast_select_fusion
  158.1 3.6 %all-to-all-start = ((bf16[16,16,1024]{2,1,0:T(8,128)(2,1)}), bf16[16,16,1024]{2,1,0:T(8,128)(2,1)S(1)}, u32[]{:S(2)}, u32[]{:S(2)}) async-start(bf16[16,16,1024]{2,1,0:T(8,128)(2,1)} %broadcast_select_fusion), calls=%async_computation.1 | async-start | bytes 1048576 | tf_op jit(solution)/shard_map/all_to_all | solution.py:125
  161.8 0.1 reduce_sum.58
  161.9 0.1 copy.51
  162.0 0.1 copy.52
  162.1 0.1 copy.57
  162.3 6.1 %all-to-all-done = bf16[16,16,1024]{2,1,0:T(8,128)(2,1)S(1)} async-done(((bf16[16,16,1024]{2,1,0:T(8,128)(2,1)}), bf16[16,16,1024]{2,1,0:T(8,128)(2,1)S(1)}, u32[]{:S(2)}, u32[]{:S(2)}) %all-to-all-start) | async-done | bytes 524320 | tf_op jit(solution)/shard_map/all_to_all | solution.py:125
  168.4 1.5 copy.82
  169.8 1.9 reshape.192
  171.8 0.2 multiply_reduce_fusion
  172.0 4.5 %convolution_multiply_fusion.2 = f32[4,16,256]{2,1,0:T(8,128)S(1)} fusion(bf16[4,4096,256]{2,1,0:T(8,128)(2,1)} %param.39, f32[4,16,4096]{2,1,0:T(8,128)S(1)} %reshape.192, f32[4096]{0:T(1024)S(1)} %convert_element_type.81, f32[4,16]{1,0:T(4,128)S(1)} %add_rsqrt_fusion), kind=kOutput, calls=%fused_computation.16 | convolution fusion | flops 134758400 | bytes 9519360 | tf_op jit(solution)/shard_map/end,edf->enf/dot_general | solution.py:131
  176.5 8.1 %fusion.12 = f32[4,16,4096]{2,1,0:T(8,128)S(1)} fusion(bf16[4,256,4096]{2,1,0:T(8,128)(2,1)} %param.41, bf16[4,4096,256]{2,1,0:T(8,128)(2,1)} %param.40, f32[4,16,4096]{2,1,0:T(8,128)S(1)} %reshape.192, f32[4096]{0:T(1024)S(1)} %convert_element_type.81, f32[4,16,256]{2,1,0:T(8,128)S(1)} %convolution_multiply_fusion.2, f32[4,16]{1,0:T(4,128)S(1)} %add_rsqrt_fusion), kind=kOutput, calls=%fused_computation.22 | convolution fusion | flops 269074432 | bytes 18956544 | tf_op jit(solution)/shard_map/enf,efd->end/dot_general | solution.py:139
  184.6 5.9 %copy.55 = f32[4,16,4096]{1,0,2:T(4,128)} copy(f32[4,16,4096]{2,1,0:T(8,128)S(1)} %fusion.12) | data formatting | bytes 2097152 | tf_op jit(solution)/shard_map/enf,efd->end/dot_general | solution.py:139
  190.5 8.8 %reshape.230 = f32[4,1,65536]{2,1,0:T(1,128)} reshape(f32[4096,4,16]{2,1,0:T(4,128)} %bitcast.60) | data formatting | bytes 2097152
  199.3 3.5 %all-to-all-start.1 = ((f32[4,1,65536]{2,1,0:T(1,128)}), f32[4,1,65536]{2,1,0:T(1,128)S(1)}, u32[]{:S(2)}, u32[]{:S(2)}) async-start(f32[4,1,65536]{2,1,0:T(1,128)} %reshape.230), calls=%async_computation.2 | async-start | bytes 2097152 | tf_op jit(solution)/shard_map/all_to_all | solution.py:140
  202.9 0.9 fusion.30
  203.8 2.2 fusion.32
  206.1 0.1 convolution_bitcast_fusion
  206.2 10.6 %all-reduce.2 = (f32[64]{0:T(128)S(1)}, f32[64]{0:T(128)S(1)}) all-reduce(f32[64]{0:T(128)S(1)} %convolution_bitcast_fusion, f32[64]{0:T(128)S(1)} %get-tuple-element.7), channel_id=1, replica_groups=mesh['ep'=4,'tp'=8] {'ep'}, use_global_device_ids=true, to_apply=%region_16.17 | all-reduce | flops 128 | bytes 1024 | tf_op jit(solution)/shard_map/psum | solution.py:90
  216.9 0.6 broadcast.214
  217.5 3.7 %reduce.5 = f32[4,65536]{1,0:T(4,128)S(1)} reduce(f32[4,1,65536]{2,1,0:T(1,128)S(1)} %all-to-all-done.1, f32[]{:T(128)} %broadcast.214), dimensions={1}, to_apply=%all_to_all.9.reduce_sub_computation | reduce | bytes 2097156 | tf_op jit(solution)/shard_map/all_to_all | solution.py:140
  221.2 9.1 %reshape.231 = f32[4096,4,16]{2,1,0:T(4,128)} reshape(f32[4,65536]{1,0:T(4,128)S(1)} %reduce.5) | data formatting | bytes 2097152
  230.3 6.7 %copy.56 = f32[4,16,4,1024]{3,1,0,2:T(8,128)S(1)} copy(f32[4,16,4,1024]{1,0,3,2:T(4,128)} %bitcast.61) | data formatting | bytes 2097152 | tf_op jit(solution)/shard_map/all_to_all | solution.py:140
  236.9 0.8 gather_fusion.1
  237.7 0.3 gather.15
  238.1 0.8 multiply_reduce_fusion.1
  238.9 11.5 %all-reduce.12.cloned.1.call-done = (f32[64,512]{1,0:T(8,128)}, f32[64,512]{1,0:T(8,128)}) async-done(((f32[64,512]{1,0:T(8,128)}, f32[64,512]{1,0:T(8,128)}), (f32[64,512]{1,0:T(8,128)}, f32[64,512]{1,0:T(8,128)})) %all-reduce.12.cloned.1.call-update) | async-done | bytes 262160 | tf_op jit(solution)/shard_map/psum | solution.py:90
  250.4 2.0 fusion.9
  252.5 55.6 %all-reduce.10.cloned.1.call-done = f32[64,1024]{1,0:T(8,128)} async-done(((f32[64,1024]{1,0:T(8,128)}), f32[64,1024]{1,0:T(8,128)}) %all-reduce.10.cloned.1.call-update) | async-done | bytes 262160 | tf_op jit(solution)/shard_map/psum | solution.py:144
  308.1 1.6 fusion.18
  (55 shorter events, 0.5 us)
Async XLA Ops:
  7.2 243.3 %copy-start = (bf16[512,1024]{1,0:T(8,128)(2,1)S(1)}, bf16[512,1024]{1,0:T(8,128)(2,1)}, u32[]{:S(2)}) copy-start(bf16[512,1024]{1,0:T(8,128)(2,1)} %param.35) | copy-start | bytes 3145732
  7.2 31.6 %reduce-scatter.2.cloned.1.call-start = ((), (), s32[]{:S(2)}) async-start(), calls=%async_computation.3 | async-start | bytes 245760 | tf_op jit(solution)/shard_map/reduce_scatter | solution.py:52
  10.5 144.4 %all-reduce.8.cloned.1.call-start = ((), (), s32[]{:S(2)}) async-start(), calls=%async_computation.4 | async-start | bytes 524288 | tf_op jit(solution)/shard_map/psum | solution.py:84
  11.6 12.3 %copy-start.10 = (s32[64]{0:T(128)S(1)}, s32[64]{0:T(128)}, u32[]{:S(2)}) copy-start(s32[64]{0:T(128)} %param.36) | copy-start | bytes 772
  11.6 12.3 %copy-start.8 = (s32[64,2]{0,1:T(2,128)S(1)}, s32[64,2]{0,1:T(2,128)}, u32[]{:S(2)}) copy-start(s32[64,2]{0,1:T(2,128)} %param.37) | copy-start | bytes 1540
  11.6 13.3 %copy-start.11 = (u32[32]{0:T(128)S(1)}, u32[32]{0:T(128)}, u32[]{:S(2)}) copy-start(u32[32]{0:T(128)} %constant.122) | copy-start | bytes 388
  24.0 20.9 %copy-start.5 = (s32[16]{0:T(128)S(1)}, s32[16]{0:T(128)}, u32[]{:S(2)}) copy-start(s32[16]{0:T(128)} %param.29) | copy-start | bytes 196
  24.0 20.9 %copy-start.6 = (f32[2]{0:T(128)S(1)}, f32[2]{0:T(128)}, u32[]{:S(2)}) copy-start(f32[2]{0:T(128)} %param.30) | copy-start | bytes 28
  44.9 53.3 %copy-start.3 = (bf16[256,1024]{1,0:T(8,128)(2,1)S(1)}, bf16[256,1024]{1,0:T(8,128)(2,1)}, u32[]{:S(2)}) copy-start(bf16[256,1024]{1,0:T(8,128)(2,1)} %param.26) | copy-start | bytes 1572868
  44.9 110.1 %copy-start.2 = (bf16[64,1024]{1,0:T(8,128)(2,1)S(1)}, bf16[64,1024]{1,0:T(8,128)(2,1)}, u32[]{:S(2)}) copy-start(bf16[64,1024]{1,0:T(8,128)(2,1)} %param.21) | copy-start | bytes 393220
  86.3 75.5 %copy-start.4 = (bf16[4096]{0:T(1024)(128)(2,1)S(1)}, bf16[4096]{0:T(1024)(128)(2,1)}, u32[]{:S(2)}) copy-start(bf16[4096]{0:T(1024)(128)(2,1)} %param.31) | copy-start | bytes 24580
  86.4 75.8 %copy-start.9 = (f32[64,2]{0,1:T(2,128)S(1)}, f32[64,2]{0,1:T(2,128)}, u32[]{:S(2)}) copy-start(f32[64,2]{0,1:T(2,128)} %param.38) | copy-start | bytes 1540
  86.4 75.8 %copy-start.7 = (bf16[1024]{0:T(1024)(128)(2,1)S(1)}, bf16[1024]{0:T(1024)(128)(2,1)}, u32[]{:S(2)}) copy-start(bf16[1024]{0:T(1024)(128)(2,1)} %param.32) | copy-start | bytes 6148
  158.1 10.3 %all-to-all-start = ((bf16[16,16,1024]{2,1,0:T(8,128)(2,1)}), bf16[16,16,1024]{2,1,0:T(8,128)(2,1)S(1)}, u32[]{:S(2)}, u32[]{:S(2)}) async-start(bf16[16,16,1024]{2,1,0:T(8,128)(2,1)} %broadcast_select_fusion), calls=%async_computation.1 | async-start | bytes 1048576 | tf_op jit(solution)/shard_map/all_to_all | solution.py:125
  184.6 18.2 %copy-start.1 = (bf16[1024,512]{1,0:T(8,128)(2,1)S(1)}, bf16[1024,512]{1,0:T(8,128)(2,1)}, u32[]{:S(2)}) copy-start(bf16[1024,512]{1,0:T(8,128)(2,1)} %param.34) | copy-start | bytes 3145732
  199.3 17.6 %all-to-all-start.1 = ((f32[4,1,65536]{2,1,0:T(1,128)}), f32[4,1,65536]{2,1,0:T(1,128)S(1)}, u32[]{:S(2)}, u32[]{:S(2)}) async-start(f32[4,1,65536]{2,1,0:T(1,128)} %reshape.230), calls=%async_computation.2 | async-start | bytes 2097152 | tf_op jit(solution)/shard_map/all_to_all | solution.py:140
  202.8 47.6 %all-reduce.12.cloned.1.call-start = ((), (), s32[]{:S(2)}) async-start(), calls=%async_computation.6 | async-start | bytes 524288 | tf_op jit(solution)/shard_map/psum | solution.py:90
  206.0 102.0 %all-reduce.10.cloned.1.call-start = ((), (), s32[]{:S(2)}) async-start(), calls=%async_computation.5 | async-start | bytes 524288 | tf_op jit(solution)/shard_map/psum | solution.py:144
Sparse Core Ops, SparseCore 0:
  10.7 26.9 reduce-scatter.1
  99.2 55.6 all-reduce.7
  207.1 43.2 all-reduce.11
  252.6 55.4 all-reduce.9
where the time goes:
time: 317 us; the launch traced here: 316 us
  waiting for transfers between devices  129 us (41%)
  local copies, waits for them, and re-layouts  52.7 us (17%)
  other arithmetic  52.6 us (17%)
  matrix products  30.5 us (10%)
  blocking collectives  29.3 us (9%)
  between operations  14.8 us (5%)
  starting transfers between devices  7.33 us (2%)
    psum x1, waiting for transfers between devices, on_device(): attn_out = lax.psum(attn_part, 'tp')  55.8 us
    psum x1, waiting for transfers between devices, on_device(): result_sum = middle_float + lax.psum(expert_part + dense_part, 'tp')  55.6 us
    another operation x3, other arithmetic  40.5 us
    unnamed x30, local copies, waits for them, and re-layouts  18.6 us
    reshape x1, local copies, waits for them, and re-layouts, on_device(): head_keys = key_cache.reshape(seq_local, cache_len, heads_local, HD)  12.3 us
    psum x1, waiting for transfers between devices, on_device(): lax.psum((jnp.dot(scaled_mid, w_dense_gate, preferred_element_type=jnp.fl...  11.5 us
    unnamed x1, blocking collectives  11.5 us
    psum x1, blocking collectives, on_device(): lax.psum((jnp.dot(scaled_mid, w_dense_gate, preferred_element_type=jnp.fl...  10.6 us
  transfers between devices with their start and end apart: 6, of which 4 were waited for; matrix products, arithmetic and copies ran while one was open for 13% of the time, Pallas kernels for 0%

commit v1 on v0

--- a/solution.py
+++ b/solution.py
@@ -81,7 +81,11 @@
         w_output,
         preferred_element_type=jnp.float32,
     )
-    attn_out = lax.psum(attn_part, "tp")
+
+    def create_the_numbers(block_here):
+        return jnp.sum(lax.all_gather(block_here, "tp"), axis=0)
+
+    attn_out = create_the_numbers(attn_part)
     middle = (tokens_float + attn_out).astype(jnp.bfloat16)
     middle_float = middle.astype(jnp.float32)
     gain_float = gain_ffn.astype(jnp.float32)

time: 317 us -> 293 us (0.924)
  waiting for transfers between devices: 129 us -> 100 us
  blocking collectives: 29.3 us -> 34 us
    psum x1 -> x0, waiting for transfers between devices: 55.8 us -> none  [on_device(): attn_out = lax.psum(attn_part, 'tp')]
    all_gather x0 -> x1, waiting for transfers between devices: none -> 27.2 us  [create_the_numbers(): return jnp.sum(lax.all_gather(block_here, 'tp'), axis=0)]
    psum x1, waiting for transfers between devices: 11.5 us -> 7.72 us  [on_device(): lax.psum((jnp.dot(scaled_mid, w_dense_gate, preferred_element_type=jnp.fl...]
    psum x1, blocking collectives: 10.6 us -> 14.4 us  [on_device(): lax.psum((jnp.dot(scaled_mid, w_dense_gate, preferred_element_type=jnp.fl...]
  transfers between devices with their start and end apart: 6 -> 6, of which waited for: 4 -> 5; matrix products, arithmetic and copies ran while one was open for 13% -> 14% of each run, Pallas kernels for 0% -> 0%
where the time goes in v1:
time: 293 us; the launch traced here: 292 us
  waiting for transfers between devices  100 us (34%)
  local copies, waits for them, and re-layouts  52.7 us (18%)
  other arithmetic  52.5 us (18%)
  blocking collectives  34 us (12%)
  matrix products  30.5 us (10%)
  between operations  14.8 us (5%)
  starting transfers between devices  7.33 us (3%)
    psum x1, waiting for transfers between devices, on_device(): result_sum = middle_float + lax.psum(expert_part + dense_part, 'tp')  55.6 us
    another operation x3, other arithmetic  40.5 us
    all_gather x1, waiting for transfers between devices, create_the_numbers(): return jnp.sum(lax.all_gather(block_here, 'tp'), axis=0)  27.2 us
    unnamed x30, local copies, waits for them, and re-layouts  18.6 us
    psum x1, blocking collectives, on_device(): lax.psum((jnp.dot(scaled_mid, w_dense_gate, preferred_element_type=jnp.fl...  14.4 us
    reshape x1, local copies, waits for them, and re-layouts, on_device(): head_keys = key_cache.reshape(seq_local, cache_len, heads_local, HD)  12.3 us
    unnamed x1, blocking collectives  11.4 us
    all_gather x1, blocking collectives, on_device(): lax.all_gather(attended, 'ep', axis=0, tiled=True)  8.16 us
  transfers between devices with their start and end apart: 6, of which 5 were waited for; matrix products, arithmetic and copies ran while one was open for 14% of the time, Pallas kernels for 0%

profile of v1, /device:TPU:0, one launch (start us, length us, event | category | flops | bytes accessed | tf_op | source)
XLA Modules:
  0.0 292.3 jit_solution(13871883810690784223)
XLA Ops:
  7.2 0.8 convert_element_type.69
  8.0 2.5 fusion.3
  10.6 12.3 %copy.64 = bf16[16,1024,256]{1,2,0:T(8,128)(2,1)} copy(bf16[16,1024,256]{2,1,0:T(8,128)(2,1)} %param.27) | data formatting | bytes 16777216 | tf_op jit(solution)/shard_map/reshape | solution.py:65
  22.9 0.6 dynamic-slice
  24.2 0.1 fusion.14
  24.3 11.4 %all-reduce.1 = f32[64]{0:T(128)S(1)} all-reduce(f32[64]{0:T(128)S(1)} %fusion.14), channel_id=4, replica_groups=mesh['ep'=4,'tp'=8] {'ep'}, use_global_device_ids=true, to_apply=%region_2.0.clone | all-reduce | flops 64 | bytes 512
  35.8 0.1 fusion.52
  35.8 1.9 reduce-scatter.2.cloned.1.call-done
  37.7 0.9 multiply_convert_fusion.6
  38.6 0.6 fusion.57
  39.2 4.6 %fusion.58 = f32[16,2,1,1024]{3,2,1,0:T(1,128)S(1)} fusion(bf16[16,2,128,1]{2,3,1,0:T(2,128)(2,1)S(1)} %reshape.227, bf16[16,1024,2,128]{1,3,2,0:T(8,128)(2,1)} %bitcast.60), kind=kOutput, calls=%fused_computation.104 | convolution fusion | flops 8388608 | bytes 8527872 | tf_op jit(solution)/shard_map/bhd,blhd->bhl/dot_general | solution.py:66
  43.8 0.4 fusion.24
  44.3 0.1 reshape.188
  44.4 39.6 %reduce-window.6 = f32[16,2,8,128]{3,2,1,0:T(8,128)S(1)} reduce-window(f32[16,2,8,128]{3,2,1,0:T(8,128)S(1)} %reshape.188, f32[]{:T(128)} %constant.94.clone.1), window={size=1x1x1x128 pad=0_0x0_0x0_0x0_127}, to_apply=%region_3.4 | reduce-window | flops 4161536 | bytes 262148 | tf_op jit(solution)/shard_map/reduce-window
  84.0 0.2 copy.48
  84.2 0.1 copy.49
  84.3 0.1 broadcast_add_fusion
  84.5 0.8 fusion.42
  85.4 4.6 %fusion = f32[16,2,1,128]{3,2,1,0:T(1,128)S(1)} fusion(bf16[16,2,1024,1]{2,1,0,3:T(2,128)(2,1)S(1)} %fusion.42, bf16[16,1024,256]{2,1,0:T(8,128)(2,1)} %param.28), kind=kOutput, calls=%fused_computation.3 | convolution fusion | flops 8388608 | bytes 8470528 | tf_op jit(solution)/shard_map/bhl,blhd->bhd/dot_general | solution.py:77
  90.0 8.2 %all_gather.9 = bf16[64,256]{1,0:T(8,128)(2,1)S(1)} all-gather(bf16[16,256]{1,0:T(8,128)(2,1)S(1)} %bitcast.72), channel_id=1, replica_groups=mesh['ep'=4,'tp'=8] {'ep'}, dimensions={0}, use_global_device_ids=true | all-gather | bytes 40960 | tf_op jit(solution)/shard_map/all_gather | solution.py:80
  98.1 0.9 fusion.59
  99.1 0.1 copy.50
  99.2 0.1 eq.19
  99.3 0.1 fusion.41
  99.4 0.1 reduce_window_sum.27
  99.5 0.2 select_reduce_fusion
  99.7 0.1 reduce_sum.69
  99.8 0.1 copy.53
  99.9 0.1 mul.169
  100.1 1.0 scatter_custom_fusion
  101.1 0.1 broadcast_in_dim.46
  101.2 27.2 %all-gather.3.cloned.1.call-done = f32[512,1024]{1,0:T(8,128)} async-done(((f32[64,1024]{1,0:T(8,128)}), f32[512,1024]{1,0:T(8,128)}) %all-gather.3.cloned.1.call-update) | async-done | bytes 2097168 | tf_op jit(solution)/shard_map/all_gather | solution.py:86
  128.4 1.7 reduce_sum.66
  130.1 0.1 fusion.17
  130.3 1.2 gather_fusion
  131.5 0.9 broadcast_select_fusion
  132.4 3.6 %all-to-all-start = ((bf16[16,16,1024]{2,1,0:T(8,128)(2,1)}), bf16[16,16,1024]{2,1,0:T(8,128)(2,1)S(1)}, u32[]{:S(2)}, u32[]{:S(2)}) async-start(bf16[16,16,1024]{2,1,0:T(8,128)(2,1)} %broadcast_select_fusion), calls=%async_computation.1 | async-start | bytes 1048576 | tf_op jit(solution)/shard_map/all_to_all | solution.py:129
  136.0 0.1 reduce_sum.68
  136.2 0.1 copy.52
  136.4 0.1 copy.57
  136.5 8.0 %all-to-all-done = bf16[16,16,1024]{2,1,0:T(8,128)(2,1)S(1)} async-done(((bf16[16,16,1024]{2,1,0:T(8,128)(2,1)}), bf16[16,16,1024]{2,1,0:T(8,128)(2,1)S(1)}, u32[]{:S(2)}, u32[]{:S(2)}) %all-to-all-start) | async-done | bytes 524320 | tf_op jit(solution)/shard_map/all_to_all | solution.py:129
  144.5 1.5 copy.82
  146.0 1.9 reshape.192
  147.9 0.2 multiply_reduce_fusion
  148.1 4.5 %convolution_multiply_fusion.2 = f32[4,16,256]{2,1,0:T(8,128)S(1)} fusion(bf16[4,4096,256]{2,1,0:T(8,128)(2,1)} %param.39, f32[4,16,4096]{2,1,0:T(8,128)S(1)} %reshape.192, f32[4096]{0:T(1024)S(1)} %convert_element_type.81, f32[4,16]{1,0:T(4,128)S(1)} %add_rsqrt_fusion), kind=kOutput, calls=%fused_computation.16 | convolution fusion | flops 134758400 | bytes 9519360 | tf_op jit(solution)/shard_map/end,edf->enf/dot_general | solution.py:135
  152.6 8.1 %fusion.12 = f32[4,16,4096]{2,1,0:T(8,128)S(1)} fusion(bf16[4,256,4096]{2,1,0:T(8,128)(2,1)} %param.41, bf16[4,4096,256]{2,1,0:T(8,128)(2,1)} %param.40, f32[4,16,4096]{2,1,0:T(8,128)S(1)} %reshape.192, f32[4096]{0:T(1024)S(1)} %convert_element_type.81, f32[4,16,256]{2,1,0:T(8,128)S(1)} %convolution_multiply_fusion.2, f32[4,16]{1,0:T(4,128)S(1)} %add_rsqrt_fusion), kind=kOutput, calls=%fused_computation.22 | convolution fusion | flops 269074432 | bytes 18956544 | tf_op jit(solution)/shard_map/enf,efd->end/dot_general | solution.py:143
  160.7 5.9 %copy.55 = f32[4,16,4096]{1,0,2:T(4,128)} copy(f32[4,16,4096]{2,1,0:T(8,128)S(1)} %fusion.12) | data formatting | bytes 2097152 | tf_op jit(solution)/shard_map/enf,efd->end/dot_general | solution.py:143
  166.6 8.8 %reshape.231 = f32[4,1,65536]{2,1,0:T(1,128)} reshape(f32[4096,4,16]{2,1,0:T(4,128)} %bitcast.61) | data formatting | bytes 2097152
  175.4 3.5 %all-to-all-start.1 = ((f32[4,1,65536]{2,1,0:T(1,128)}), f32[4,1,65536]{2,1,0:T(1,128)S(1)}, u32[]{:S(2)}, u32[]{:S(2)}) async-start(f32[4,1,65536]{2,1,0:T(1,128)} %reshape.231), calls=%async_computation.2 | async-start | bytes 2097152 | tf_op jit(solution)/shard_map/all_to_all | solution.py:144
  179.0 0.9 fusion.30
  179.9 2.2 fusion.32
  182.2 0.1 convolution_bitcast_fusion
  182.3 14.4 %all-reduce.2 = (f32[64]{0:T(128)S(1)}, f32[64]{0:T(128)S(1)}) all-reduce(f32[64]{0:T(128)S(1)} %convolution_bitcast_fusion, f32[64]{0:T(128)S(1)} %get-tuple-element.7), channel_id=1, replica_groups=mesh['ep'=4,'tp'=8] {'ep'}, use_global_device_ids=true, to_apply=%region_16.17 | all-reduce | flops 128 | bytes 1024 | tf_op jit(solution)/shard_map/psum | solution.py:94
  196.8 0.6 broadcast.214
  197.4 3.7 %reduce.5 = f32[4,65536]{1,0:T(4,128)S(1)} reduce(f32[4,1,65536]{2,1,0:T(1,128)S(1)} %all-to-all-done.1, f32[]{:T(128)} %broadcast.214), dimensions={1}, to_apply=%all_to_all.9.reduce_sub_computation | reduce | bytes 2097156 | tf_op jit(solution)/shard_map/all_to_all | solution.py:144
  201.1 9.1 %reshape.232 = f32[4096,4,16]{2,1,0:T(4,128)} reshape(f32[4,65536]{1,0:T(4,128)S(1)} %reduce.5) | data formatting | bytes 2097152
  210.2 6.7 %copy.56 = f32[4,16,4,1024]{3,1,0,2:T(8,128)S(1)} copy(f32[4,16,4,1024]{1,0,3,2:T(4,128)} %bitcast.62) | data formatting | bytes 2097152 | tf_op jit(solution)/shard_map/all_to_all | solution.py:144
  216.8 0.8 gather_fusion.1
  217.6 0.3 gather.15
  218.0 0.8 multiply_reduce_fusion.1
  218.8 7.7 %all-reduce.9.cloned.1.call-done = (f32[64,512]{1,0:T(8,128)}, f32[64,512]{1,0:T(8,128)}) async-done(((f32[64,512]{1,0:T(8,128)}, f32[64,512]{1,0:T(8,128)}), (f32[64,512]{1,0:T(8,128)}, f32[64,512]{1,0:T(8,128)})) %all-reduce.9.cloned.1.call-update) | async-done | bytes 262160 | tf_op jit(solution)/shard_map/psum | solution.py:94
  226.5 2.0 fusion.9
  228.5 55.6 %all-reduce.7.cloned.1.call-done = f32[64,1024]{1,0:T(8,128)} async-done(((f32[64,1024]{1,0:T(8,128)}), f32[64,1024]{1,0:T(8,128)}) %all-reduce.7.cloned.1.call-update) | async-done | bytes 262160 | tf_op jit(solution)/shard_map/psum | solution.py:148
  284.1 1.6 fusion.18
  (56 shorter events, 0.6 us)
Async XLA Ops:
  7.2 219.3 %copy-start = (bf16[512,1024]{1,0:T(8,128)(2,1)S(1)}, bf16[512,1024]{1,0:T(8,128)(2,1)}, u32[]{:S(2)}) copy-start(bf16[512,1024]{1,0:T(8,128)(2,1)} %param.35) | copy-start | bytes 3145732
  7.2 30.6 %reduce-scatter.2.cloned.1.call-start = ((), (), s32[]{:S(2)}) async-start(), calls=%async_computation.3 | async-start | bytes 245760 | tf_op jit(solution)/shard_map/reduce_scatter | solution.py:52
  10.5 117.9 %all-gather.3.cloned.1.call-start = ((), (), s32[]{:S(2)}) async-start(), calls=%async_computation.5 | async-start | bytes 2359296 | tf_op jit(solution)/shard_map/all_gather | solution.py:86
  10.6 12.4 %copy-start.11 = (u32[32]{0:T(128)S(1)}, u32[32]{0:T(128)}, u32[]{:S(2)}) copy-start(u32[32]{0:T(128)} %constant.122) | copy-start | bytes 388
  10.6 13.6 %copy-start.2 = (bf16[64,1024]{1,0:T(8,128)(2,1)S(1)}, bf16[64,1024]{1,0:T(8,128)(2,1)}, u32[]{:S(2)}) copy-start(bf16[64,1024]{1,0:T(8,128)(2,1)} %param.21) | copy-start | bytes 393220
  22.9 20.9 %copy-start.5 = (s32[16]{0:T(128)S(1)}, s32[16]{0:T(128)}, u32[]{:S(2)}) copy-start(s32[16]{0:T(128)} %param.29) | copy-start | bytes 196
  22.9 20.9 %copy-start.6 = (f32[2]{0:T(128)S(1)}, f32[2]{0:T(128)}, u32[]{:S(2)}) copy-start(f32[2]{0:T(128)} %param.30) | copy-start | bytes 28
  43.8 54.3 %copy-start.3 = (bf16[256,1024]{1,0:T(8,128)(2,1)S(1)}, bf16[256,1024]{1,0:T(8,128)(2,1)}, u32[]{:S(2)}) copy-start(bf16[256,1024]{1,0:T(8,128)(2,1)} %param.26) | copy-start | bytes 1572868
  43.8 55.3 %copy-start.10 = (s32[64]{0:T(128)S(1)}, s32[64]{0:T(128)}, u32[]{:S(2)}) copy-start(s32[64]{0:T(128)} %param.36) | copy-start | bytes 772
  43.8 55.3 %copy-start.8 = (s32[64,2]{0,1:T(2,128)S(1)}, s32[64,2]{0,1:T(2,128)}, u32[]{:S(2)}) copy-start(s32[64,2]{0,1:T(2,128)} %param.37) | copy-start | bytes 1540
  85.3 50.8 %copy-start.4 = (bf16[4096]{0:T(1024)(128)(2,1)S(1)}, bf16[4096]{0:T(1024)(128)(2,1)}, u32[]{:S(2)}) copy-start(bf16[4096]{0:T(1024)(128)(2,1)} %param.31) | copy-start | bytes 24580
  85.3 51.0 %copy-start.9 = (f32[64,2]{0,1:T(2,128)S(1)}, f32[64,2]{0,1:T(2,128)}, u32[]{:S(2)}) copy-start(f32[64,2]{0,1:T(2,128)} %param.38) | copy-start | bytes 1540
  85.3 51.1 %copy-start.7 = (bf16[1024]{0:T(1024)(128)(2,1)S(1)}, bf16[1024]{0:T(1024)(128)(2,1)}, u32[]{:S(2)}) copy-start(bf16[1024]{0:T(1024)(128)(2,1)} %param.32) | copy-start | bytes 6148
  132.4 12.1 %all-to-all-start = ((bf16[16,16,1024]{2,1,0:T(8,128)(2,1)}), bf16[16,16,1024]{2,1,0:T(8,128)(2,1)S(1)}, u32[]{:S(2)}, u32[]{:S(2)}) async-start(bf16[16,16,1024]{2,1,0:T(8,128)(2,1)} %broadcast_select_fusion), calls=%async_computation.1 | async-start | bytes 1048576 | tf_op jit(solution)/shard_map/all_to_all | solution.py:129
  160.7 18.2 %copy-start.1 = (bf16[1024,512]{1,0:T(8,128)(2,1)S(1)}, bf16[1024,512]{1,0:T(8,128)(2,1)}, u32[]{:S(2)}) copy-start(bf16[1024,512]{1,0:T(8,128)(2,1)} %param.34) | copy-start | bytes 3145732
  175.4 21.3 %all-to-all-start.1 = ((f32[4,1,65536]{2,1,0:T(1,128)}), f32[4,1,65536]{2,1,0:T(1,128)S(1)}, u32[]{:S(2)}, u32[]{:S(2)}) async-start(f32[4,1,65536]{2,1,0:T(1,128)} %reshape.231), calls=%async_computation.2 | async-start | bytes 2097152 | tf_op jit(solution)/shard_map/all_to_all | solution.py:144
  178.9 47.6 %all-reduce.9.cloned.1.call-start = ((), (), s32[]{:S(2)}) async-start(), calls=%async_computation.6 | async-start | bytes 524288 | tf_op jit(solution)/shard_map/psum | solution.py:94
  182.1 102.0 %all-reduce.7.cloned.1.call-start = ((), (), s32[]{:S(2)}) async-start(), calls=%async_computation.4 | async-start | bytes 524288 | tf_op jit(solution)/shard_map/psum | solution.py:148
Sparse Core Ops, SparseCore 0:
  10.7 26.9 reduce-scatter.1
  99.2 29.1 all-gather.2
  183.2 43.2 all-reduce.8
  228.7 55.4 all-reduce.6
